TPU v7x, 32 devices: a whole 2x2x4 slice. The times are simulated.
32 devices in a mesh: sp: 8 (over z, y), tp: 4 (over x, core).
Axes of the slice: x: 2, y: 2, z: 4, core: 2. Of those that a mesh axis runs over, the one named last changes fastest.
Arguments:
- q_proj: bfloat16 [4096, 1024], P('sp', 'tp'), may hold values from -5.25 to 5.25
- k_proj: bfloat16 [4096, 512], P('sp', 'tp'), may hold values from -5.25 to 5.25
- v_proj: bfloat16 [4096, 512], P('sp', 'tp'), may hold values from -6 to 6
- doc_ids: int32 [4096], P('sp'), may hold values from 0 to 3, never falling along the last dimension, each value on 1 to 2048 neighbouring positions
- sinks: float32 [16], P('tp'), may hold values from 0.5 to 5.5
- resid: bfloat16 [4096, 2048], P(('sp', 'tp')), may hold values from -12 to 12
- w_out: bfloat16 [1024, 2048], P('tp'), may hold values from -4 to 4
- norm_gain: float32 [2048], replicated, may hold values from 0.1 to 1.9
- w_gate: bfloat16 [2048, 5632], P('sp', 'tp'), may hold values from -0.125 to 0.125
- w_up: bfloat16 [2048, 5632], P('sp', 'tp'), may hold values from -0.125 to 0.125
- w_down: bfloat16 [5632, 2048], P('tp', 'sp'), may hold values from -0.078125 to 0.078125
Outputs:
- layer_out: bfloat16 [4096, 2048], P(('sp', 'tp'))
Inputs may be any that keep to these rules, and one draw needn't show every extreme that they name: `doc_ids`: document numbers never fall along the sequence; each document covers at most 2048 positions and one covers exactly that many.
All inputs are finite; a program needn't handle non-finite values.
Results may differ from a plain program's by a relative error of at most 0.015.
Values may be sent and summed in bfloat16 or wider, within the bound.
No kernel may reach another device: no remote copies, remote signals or barrier semaphores. Data moves between devices by JAX's collectives and lax.ppermute only.
A program may use at most 64 MiB of HBM per device.

v0:
```python
import jax
import jax.numpy as jnp
from jax import lax
from jax.sharding import PartitionSpec as P

HEAD = 64
WINDOW = 128
norm_eps = 1e-06
masked = -1e30


def with_halo(block, sides, width):
    for axis, dim in sides:
        count = lax.axis_size(axis)
        forward = [(i, i + 1) for i in range(count - 1)]
        backward = [(target, source) for source, target in forward]
        low = lax.ppermute(
            lax.slice_in_dim(block, block.shape[dim] - width, None, axis=dim), axis, forward
        )
        high = lax.ppermute(lax.slice_in_dim(block, 0, width, axis=dim), axis, backward)
        block = jnp.concatenate([low, block, high], axis=dim)
    return block


def normalize(middle, norm_gain):
    return (
        middle * lax.rsqrt(jnp.mean(middle * middle, axis=-1, keepdims=True) + norm_eps) * norm_gain
    ).astype(jnp.bfloat16)


def band_view(extended, block_count):
    shaped = extended.reshape((block_count + 2, WINDOW) + extended.shape[1:])
    return jnp.concatenate([shaped[:-2], shaped[1:-1], shaped[2:]], axis=1)


def shards(q_proj, k_proj, v_proj, doc_ids, sinks, resid, w_out, norm_gain, w_gate, w_up, w_down):
    tok_rows = q_proj.shape[0]
    kv_local = k_proj.shape[1] // HEAD
    groups = q_proj.shape[1] // HEAD // kv_local
    block_count = tok_rows // WINDOW
    full_out = lax.all_gather(w_out, "tp", axis=0, tiled=True)
    keys_ext, values_ext, docs_ext = (
        with_halo(k_proj, (("sp", 0),), WINDOW),
        with_halo(v_proj, (("sp", 0),), WINDOW),
        with_halo(doc_ids, (("sp", 0),), WINDOW),
    )
    positions = (
        lax.axis_index("sp") * tok_rows
        - WINDOW
        + jnp.arange(tok_rows + 2 * WINDOW, dtype=jnp.int32)
    )
    inside = (positions >= 0) & (positions < tok_rows * lax.axis_size("sp"))
    docs_ext = jnp.where(inside, docs_ext, -1)
    key_band = band_view(keys_ext.reshape(tok_rows + 2 * WINDOW, kv_local, HEAD), block_count)
    value_band = band_view(values_ext.reshape(tok_rows + 2 * WINDOW, kv_local, HEAD), block_count)
    doc_band = band_view(docs_ext, block_count)
    queries = q_proj.reshape(block_count, WINDOW, kv_local, groups, HEAD)
    scores = jnp.einsum(
        "bqhgd,bkhd->bhgqk", queries, key_band, preferred_element_type=jnp.float32
    ) * HEAD ** (-0.5)
    offsets = jnp.arange(3 * WINDOW, dtype=jnp.int32) - WINDOW
    near = jnp.abs(jnp.arange(WINDOW, dtype=jnp.int32)[:, None] - offsets[None, :]) <= WINDOW
    query_docs = doc_ids.reshape(block_count, WINDOW)
    valid = near[None] & (query_docs[:, :, None] == doc_band[:, None, :])
    scores = jnp.where(valid[:, None, None], scores, masked)
    sink_table = sinks.reshape(kv_local, groups)[None, :, :, None, None]
    top = jnp.maximum(jnp.max(scores, axis=-1, keepdims=True), sink_table)
    expd = jnp.exp(scores - top)
    probs = (expd / (jnp.sum(expd, axis=-1, keepdims=True) + jnp.exp(sink_table - top))).astype(
        jnp.bfloat16
    )
    attended = jnp.einsum(
        "bhgqk,bkhd->bqhgd", probs, value_band, preferred_element_type=jnp.float32
    )
    attended = attended.astype(jnp.bfloat16).reshape(tok_rows, kv_local * groups * HEAD)
    own_rows = lax.all_to_all(attended, "tp", split_axis=0, concat_axis=1, tiled=True)
    projected = jnp.dot(own_rows, full_out, preferred_element_type=jnp.float32)
    middle = resid.astype(jnp.float32) + projected
    normed = lax.all_gather(normalize(middle, norm_gain), "tp", axis=0, tiled=True)

    def add_rows(piece):
        return jnp.dot(normed, piece, preferred_element_type=jnp.float32)

    gate = add_rows(lax.all_gather(w_gate, "sp", axis=0, tiled=True))
    up_part = add_rows(lax.all_gather(w_up, "sp", axis=0, tiled=True))
    hidden = (jax.nn.silu(gate) * up_part).astype(jnp.bfloat16)
    down_full = lax.all_gather(w_down, "sp", axis=1, tiled=True)
    summed_down = lax.psum_scatter(
        jnp.dot(hidden, down_full, preferred_element_type=jnp.float32).astype(jnp.bfloat16),
        "tp",
        scatter_dimension=0,
        tiled=True,
    ).astype(jnp.float32)
    return (middle + summed_down).astype(jnp.bfloat16)


def solution(mesh):
    placed = (
        P("sp", "tp"),
        P("sp", "tp"),
        P("sp", "tp"),
        P("sp"),
        P("tp"),
        P(("sp", "tp"), None),
        P("tp", None),
        P(),
        P("sp", "tp"),
        P("sp", "tp"),
        P("tp", "sp"),
    )
    return jax.shard_map(
        shards, mesh=mesh, in_specs=placed, out_specs=P(("sp", "tp"), None), check_vma=False
    )
```

profile of v0, /device:TPU:0, one launch (start us, length us, event | category | flops | bytes accessed | tf_op | source)
XLA Modules:
  0.0 408.3 jit_solution(3084332801912330174)
XLA Ops:
  6.6 0.7 all-gather.6.cloned.1.call-update
  7.3 0.8 fusion.27
  8.1 4.9 %collective-permute-start.2 = (s32[128]{0:T(128)S(1)}, s32[128]{0:T(128)S(1)}, u32[]{:S(2)}, u32[]{:S(2)}) collective-permute-start(s32[128]{0:T(128)S(1)} %get-tuple-element.16), channel_id=1, source_target_pairs={{0,4},{4,8},{8,12},{12,16},{16,20},{20,24},{24,28},{1,5},{5,9},{9,... | collective-permute-start | bytes 1544 | tf_op jit(solution)/shard_map/ppermute | solution.py:17
  13.0 1.3 collective-permute-start.3
  14.3 0.8 fusion.25
  15.1 4.5 %collective-permute-start.4 = (bf16[128,128]{1,0:T(8,128)(2,1)S(1)}, bf16[128,128]{1,0:T(8,128)(2,1)S(1)}, u32[]{:S(2)}, u32[]{:S(2)}) collective-permute-start(bf16[128,128]{1,0:T(8,128)(2,1)S(1)} %get-tuple-element.11), channel_id=1, source_target_pairs={{0,4},{4,8},{8,12},{12,16},{16,20},{20,24},{24,28},{1,5},{5,9},{9,... | collective-permute-start | bytes 98312 | tf_op jit(solution)/shard_map/ppermute | solution.py:17
  19.6 1.3 collective-permute-start.5
  20.9 0.8 fusion.24
  21.7 4.9 %collective-permute-start = (bf16[128,128]{1,0:T(8,128)(2,1)S(1)}, bf16[128,128]{1,0:T(8,128)(2,1)S(1)}, u32[]{:S(2)}, u32[]{:S(2)}) collective-permute-start(bf16[128,128]{1,0:T(8,128)(2,1)S(1)} %get-tuple-element.7), channel_id=1, source_target_pairs={{0,4},{4,8},{8,12},{12,16},{16,20},{20,24},{24,28},{1,5},{5,9},{9,... | collective-permute-start | bytes 98312 | tf_op jit(solution)/shard_map/ppermute | solution.py:17
  26.6 1.0 reshape.90
  27.7 1.0 reshape.87
  28.9 1.2 reshape.92
  30.5 1.3 collective-permute-start.1
  31.9 0.3 compare_and_fusion
  32.8 4.4 %collective-permute-done.1 = bf16[128,128]{1,0:T(8,128)(2,1)S(1)} collective-permute-done((bf16[128,128]{1,0:T(8,128)(2,1)S(1)}, bf16[128,128]{1,0:T(8,128)(2,1)S(1)}, u32[]{:S(2)}, u32[]{:S(2)}) %collective-permute-start.1) | collective-permute-done | bytes 32800 | tf_op jit(solution)/shard_map/ppermute | solution.py:20
  37.8 0.7 fusion.2
  38.6 0.7 fusion.1
  39.4 1.0 fusion.4
  40.4 8.6 %all_to_all.19 = bf16[4,128,256]{1,2,0:T(8,128)(2,1)S(1)} all-to-all(bf16[4,128,256]{1,2,0:T(8,128)(2,1)S(1)} %bitcast.42), channel_id=1, replica_groups=mesh['sp'=8,'tp'=4] {'tp'}, dimensions={0} | all-to-all | bytes 524288 | tf_op jit(solution)/shard_map/all_to_all | solution.py:76
  49.0 3.0 multiply_reduce_fusion
  52.0 1.0 multiply_convert_fusion
  53.0 0.7 all-gather.10.cloned.1.call-update
  53.7 0.5 all-gather.12.cloned.1.call-update
  54.3 0.5 all-gather.14.cloned.1.call-update
  55.1 21.3 %all-gather.8.cloned.1.call-done = bf16[512,2048]{1,0:T(8,128)(2,1)} async-done(((bf16[128,2048]{1,0:T(8,128)(2,1)}), bf16[512,2048]{1,0:T(8,128)(2,1)}) %all-gather.8.cloned.1.call-update) | async-done | bytes 2097168 | tf_op jit(solution)/shard_map/all_gather | solution.py:79
  76.4 94.5 %all-gather.10.cloned.1.call-done = bf16[2048,1408]{1,0:T(8,128)(2,1)} async-done(((bf16[256,1408]{1,0:T(8,128)(2,1)}), bf16[2048,1408]{1,0:T(8,128)(2,1)}) %all-gather.10.cloned.1.call-update) | async-done | bytes 5767184 | tf_op jit(solution)/shard_map/all_gather | solution.py:84
  170.9 8.3 %fusion.28 = f32[512,1408]{1,0:T(8,128)} fusion(bf16[512,2048]{1,0:T(8,128)(2,1)} %all-gather.8.cloned.1.call-done, bf16[2048,1408]{1,0:T(8,128)(2,1)} %all-gather.10.cloned.1.call-done), kind=kOutput, calls=%fused_computation.52 | convolution fusion | flops 2952790016 | bytes 10747904 | tf_op jit(solution)/shard_map/dot_general | solution.py:82
  179.2 84.3 %all-gather.12.cloned.1.call-done = bf16[2048,1408]{1,0:T(8,128)(2,1)} async-done(((bf16[256,1408]{1,0:T(8,128)(2,1)}), bf16[2048,1408]{1,0:T(8,128)(2,1)}) %all-gather.12.cloned.1.call-update) | async-done | bytes 5767184 | tf_op jit(solution)/shard_map/all_gather | solution.py:85
  263.5 93.2 %all-gather.14.cloned.1.call-done = bf16[1408,2048]{1,0:T(8,128)(2,1)} async-done(((bf16[1408,256]{1,0:T(8,128)(2,1)}), bf16[1408,2048]{1,0:T(8,128)(2,1)}) %all-gather.14.cloned.1.call-update) | async-done | bytes 5767184 | tf_op jit(solution)/shard_map/all_gather | solution.py:87
  356.7 13.3 %convolution_convert_fusion = bf16[512,2048]{1,0:T(8,128)(2,1)} fusion(bf16[1408,2048]{1,0:T(8,128)(2,1)} %all-gather.14.cloned.1.call-done, bf16[512,2048]{1,0:T(8,128)(2,1)S(1)} %copy-done.5, bf16[2048,1408]{1,0:T(8,128)(2,1)} %all-gather.12.cloned.1.call-done, f32[512,1408]{1,0:T(8,128)} %fusion.28), kind=kOutput, calls=%fused_computation.5 | convolution fusion | flops 5910953984 | bytes 18612224 | tf_op jit(solution)/shard_map/dot_general | solution.py:89
  370.0 29.5 %reduce-scatter.2.cloned.1.call-done = bf16[128,2048]{1,0:T(8,128)(2,1)} async-done(((bf16[512,2048]{1,0:T(8,128)(2,1)}), bf16[128,2048]{1,0:T(8,128)(2,1)}) %reduce-scatter.2.cloned.1.call-update) | async-done | bytes 524304 | tf_op jit(solution)/shard_map/reduce_scatter | solution.py:88
  399.5 1.9 add_convert_fusion
  (49 shorter events, 2.3 us)
Async XLA Ops:
  6.5 25.3 %copy-start.3 = (s32[512]{0:T(512)S(1)}, s32[512]{0:T(512)}, u32[]{:S(2)}) copy-start(s32[512]{0:T(512)} %param.14) | copy-start | bytes 6148
  6.5 25.6 %copy-start = (bf16[512,128]{1,0:T(8,128)(2,1)S(1)}, bf16[512,128]{1,0:T(8,128)(2,1)}, u32[]{:S(2)}) copy-start(bf16[512,128]{1,0:T(8,128)(2,1)} %param.12) | copy-start | bytes 393220
  6.5 30.7 %copy-start.1 = (bf16[512,128]{1,0:T(8,128)(2,1)S(1)}, bf16[512,128]{1,0:T(8,128)(2,1)}, u32[]{:S(2)}) copy-start(bf16[512,128]{1,0:T(8,128)(2,1)} %param.13) | copy-start | bytes 393220
  6.5 23.7 %copy-start.6 = (f32[4]{0:T(128)S(1)}, f32[4]{0:T(128)}, u32[]{:S(2)}) copy-start(f32[4]{0:T(128)} %param.15) | copy-start | bytes 52
  6.5 42.4 %all-gather.6.cloned.1.call-start = ((), (), s32[]{:S(2)}) async-start(), calls=%async_computation.2 | async-start | bytes 5242880 | tf_op jit(solution)/shard_map/all_gather | solution.py:41
  7.3 69.1 %all-gather.8.cloned.1.call-start = ((), (), s32[]{:S(2)}) async-start(), calls=%async_computation.3 | async-start | bytes 2621440 | tf_op jit(solution)/shard_map/all_gather | solution.py:79
  8.1 22.4 %collective-permute-start.2 = (s32[128]{0:T(128)S(1)}, s32[128]{0:T(128)S(1)}, u32[]{:S(2)}, u32[]{:S(2)}) collective-permute-start(s32[128]{0:T(128)S(1)} %get-tuple-element.16), channel_id=1, source_target_pairs={{0,4},{4,8},{8,12},{12,16},{16,20},{20,24},{24,28},{1,5},{5,9},{9,... | collective-permute-start | bytes 1544 | tf_op jit(solution)/shard_map/ppermute | solution.py:17
  13.0 18.8 %collective-permute-start.3 = (s32[128]{0:T(128)S(1)}, s32[128]{0:T(128)S(1)}, u32[]{:S(2)}, u32[]{:S(2)}) collective-permute-start(s32[128]{0:T(128)S(1)} %get-tuple-element.17), channel_id=1, source_target_pairs={{4,0},{8,4},{12,8},{16,12},{20,16},{24,20},{28,24},{5,1},{9,5},{13... | collective-permute-start | bytes 1544 | tf_op jit(solution)/shard_map/ppermute | solution.py:20
  15.1 17.1 %collective-permute-start.4 = (bf16[128,128]{1,0:T(8,128)(2,1)S(1)}, bf16[128,128]{1,0:T(8,128)(2,1)S(1)}, u32[]{:S(2)}, u32[]{:S(2)}) collective-permute-start(bf16[128,128]{1,0:T(8,128)(2,1)S(1)} %get-tuple-element.11), channel_id=1, source_target_pairs={{0,4},{4,8},{8,12},{12,16},{16,20},{20,24},{24,28},{1,5},{5,9},{9,... | collective-permute-start | bytes 98312 | tf_op jit(solution)/shard_map/ppermute | solution.py:17
  19.6 12.6 %collective-permute-start.5 = (bf16[128,128]{1,0:T(8,128)(2,1)S(1)}, bf16[128,128]{1,0:T(8,128)(2,1)S(1)}, u32[]{:S(2)}, u32[]{:S(2)}) collective-permute-start(bf16[128,128]{1,0:T(8,128)(2,1)S(1)} %get-tuple-element.12), channel_id=1, source_target_pairs={{4,0},{8,4},{12,8},{16,12},{20,16},{24,20},{28,24},{5,1},{9,5},{13... | collective-permute-start | bytes 98312 | tf_op jit(solution)/shard_map/ppermute | solution.py:20
  21.7 11.1 %collective-permute-start = (bf16[128,128]{1,0:T(8,128)(2,1)S(1)}, bf16[128,128]{1,0:T(8,128)(2,1)S(1)}, u32[]{:S(2)}, u32[]{:S(2)}) collective-permute-start(bf16[128,128]{1,0:T(8,128)(2,1)S(1)} %get-tuple-element.7), channel_id=1, source_target_pairs={{0,4},{4,8},{8,12},{12,16},{16,20},{20,24},{24,28},{1,5},{5,9},{9,... | collective-permute-start | bytes 98312 | tf_op jit(solution)/shard_map/ppermute | solution.py:17
  30.5 6.7 %collective-permute-start.1 = (bf16[128,128]{1,0:T(8,128)(2,1)S(1)}, bf16[128,128]{1,0:T(8,128)(2,1)S(1)}, u32[]{:S(2)}, u32[]{:S(2)}) collective-permute-start(bf16[128,128]{1,0:T(8,128)(2,1)S(1)} %get-tuple-element.8), channel_id=1, source_target_pairs={{4,0},{8,4},{12,8},{16,12},{20,16},{24,20},{28,24},{5,1},{9,5},{13... | collective-permute-start | bytes 98312 | tf_op jit(solution)/shard_map/ppermute | solution.py:20
  39.4 9.6 %copy-start.2 = (bf16[128,2048]{1,0:T(8,128)(2,1)S(1)}, bf16[128,2048]{1,0:T(8,128)(2,1)}, u32[]{:S(2)}) copy-start(bf16[128,2048]{1,0:T(8,128)(2,1)} %param.16) | copy-start | bytes 1572868
  48.9 3.0 copy-start.4
  53.0 117.9 %all-gather.10.cloned.1.call-start = ((), (), s32[]{:S(2)}) async-start(), calls=%async_computation.4 | async-start | bytes 6488064 | tf_op jit(solution)/shard_map/all_gather | solution.py:84
  53.7 209.8 %all-gather.12.cloned.1.call-start = ((), (), s32[]{:S(2)}) async-start(), calls=%async_computation.5 | async-start | bytes 6488064 | tf_op jit(solution)/shard_map/all_gather | solution.py:85
  54.3 302.4 %all-gather.14.cloned.1.call-start = ((), (), s32[]{:S(2)}) async-start(), calls=%async_computation.6 | async-start | bytes 6488064 | tf_op jit(solution)/shard_map/all_gather | solution.py:87
  54.9 344.6 %reduce-scatter.2.cloned.1.call-start = ((), (), s32[]{:S(2)}) async-start(), calls=%async_computation.7 | async-start | bytes 2621440 | tf_op jit(solution)/shard_map/reduce_scatter | solution.py:88
  76.4 280.3 %copy-start.5 = (bf16[512,2048]{1,0:T(8,128)(2,1)S(1)}, bf16[512,2048]{1,0:T(8,128)(2,1)}, u32[]{:S(2)}) copy-start(bf16[512,2048]{1,0:T(8,128)(2,1)} %all-gather.8.cloned.1.call-done) | copy-start | bytes 6291460
Sparse Core Ops, SparseCore 0:
  8.9 37.1 all-gather.5
  53.1 23.2 all-gather.7
  78.5 92.3 all-gather.9
  172.9 90.4 all-gather.11
  265.3 91.2 all-gather.13
  370.1 29.3 reduce-scatter.1
where the time goes:
time: 409 us; the launch traced here: 408 us
  waiting for transfers between devices  330 us (81%)
  matrix products  26.2 us (6%)
  starting transfers between devices  18.6 us (5%)
  between operations  13.8 us (3%)
  blocking collectives  8.59 us (2%)
  local copies, waits for them, and re-layouts  7.14 us (2%)
  other arithmetic  4.2 us (1%)
    all_gather x1, waiting for transfers between devices, shards(): gate = add_rows(lax.all_gather(w_gate, 'sp', axis=0, tiled=True))  94.5 us
    all_gather x1, waiting for transfers between devices, shards(): down_full = lax.all_gather(w_down, 'sp', axis=1, tiled=True)  93.2 us
    all_gather x1, waiting for transfers between devices, shards(): up_part = add_rows(lax.all_gather(w_up, 'sp', axis=0, tiled=True))  84.3 us
    reduce_scatter x1, waiting for transfers between devices, shards(): lax.psum_scatter(jnp.dot(hidden, down_full, preferred_element_type=jnp.fl...  29.5 us
    all_gather x1, waiting for transfers between devices, shards(): lax.all_gather(normalize(middle, norm_gain), 'tp', axis=0, tiled=True)  21.3 us
    ppermute x3, starting transfers between devices, with_halo(): lax.ppermute(lax.slice_in_dim(block, block.shape[dim] - width, None, axis...  14.4 us
    dot_general x1, matrix products, shards(): jnp.dot(hidden, down_full, preferred_element_type=jnp.float32)  13.3 us
    all_to_all x1, blocking collectives, shards(): lax.all_to_all(attended, 'tp', split_axis=0, concat_axis=1, tiled=True)  8.59 us
  transfers between devices with their start and end apart: 12, of which 6 were waited for; matrix products, arithmetic and copies ran while one was open for 4% of the time, Pallas kernels for 0%

commit v1 on v0

--- a/solution.py
+++ b/solution.py
@@ -84,7 +84,12 @@
     gate = add_rows(lax.all_gather(w_gate, "sp", axis=0, tiled=True))
     up_part = add_rows(lax.all_gather(w_up, "sp", axis=0, tiled=True))
     hidden = (jax.nn.silu(gate) * up_part).astype(jnp.bfloat16)
-    down_full = lax.all_gather(w_down, "sp", axis=1, tiled=True)
+    ring = [w_down]
+    for hop in range(7):
+        ring.append(lax.ppermute(ring[-1], "sp", [(dev, (dev + 1) % 8) for dev in range(8)]))
+    down_full = jnp.roll(
+        jnp.concatenate(ring[::-1], axis=1), (lax.axis_index("sp") + 1) * ring[0].shape[1], axis=1
+    )
     summed_down = lax.psum_scatter(
         jnp.dot(hidden, down_full, preferred_element_type=jnp.float32).astype(jnp.bfloat16),
         "tp",

time: 409 us -> 374 us (0.914)
  waiting for transfers between devices: 330 us -> 262 us
  local copies, waits for them, and re-layouts: 7.14 us -> 32.8 us
    ppermute x0 -> x7, waiting for transfers between devices: none -> 191 us  [shards(): lax.ppermute(ring[-1], 'sp', [(dev, (dev + 1) % 8) for dev in range(8)])]
    all_gather x1, waiting for transfers between devices: 94.5 us -> 0.01 us  [shards(): gate = add_rows(lax.all_gather(w_gate, 'sp', axis=0, tiled=True))]
    all_gather x1 -> x0, waiting for transfers between devices: 93.2 us -> none  [shards(): down_full = lax.all_gather(w_down, 'sp', axis=1, tiled=True)]
    all_gather x1, waiting for transfers between devices: 84.3 us -> 38.1 us  [shards(): up_part = add_rows(lax.all_gather(w_up, 'sp', axis=0, tiled=True))]
    unnamed x14 -> x37, local copies, waits for them, and re-layouts: 0.03 us -> 24 us
    all_gather x1, waiting for transfers between devices: 21.3 us -> 0.01 us  [shards(): lax.all_gather(normalize(middle, norm_gain), 'tp', axis=0, tiled=True)]
  transfers between devices with their start and end apart: 12 -> 18, of which waited for: 6 -> 10; matrix products, arithmetic and copies ran while one was open for 4% -> 12% of each run, Pallas kernels for 0% -> 0%
where the time goes in v1:
time: 374 us; the launch traced here: 373 us
  waiting for transfers between devices  262 us (70%)
  local copies, waits for them, and re-layouts  32.8 us (9%)
  matrix products  26.4 us (7%)
  starting transfers between devices  22.5 us (6%)
  between operations  13.5 us (4%)
  blocking collectives  8.71 us (2%)
  other arithmetic  6.53 us (2%)
    ppermute x7, waiting for transfers between devices, shards(): lax.ppermute(ring[-1], 'sp', [(dev, (dev + 1) % 8) for dev in range(8)])  191 us
    all_gather x1, waiting for transfers between devices, shards(): up_part = add_rows(lax.all_gather(w_up, 'sp', axis=0, tiled=True))  38.1 us
    reduce_scatter x1, waiting for transfers between devices, shards(): lax.psum_scatter(jnp.dot(hidden, down_full, preferred_element_type=jnp.fl...  29.5 us
    unnamed x37, local copies, waits for them, and re-layouts  24 us
    ppermute x3, starting transfers between devices, with_halo(): lax.ppermute(lax.slice_in_dim(block, block.shape[dim] - width, None, axis...  14.9 us
    dot_general x1, matrix products, shards(): jnp.dot(hidden, down_full, preferred_element_type=jnp.float32)  13.2 us
    all_to_all x1, blocking collectives, shards(): lax.all_to_all(attended, 'tp', split_axis=0, concat_axis=1, tiled=True)  8.71 us
    dot_general x1, matrix products, add_rows(): return jnp.dot(normed, piece, preferred_element_type=jnp.float32)  8.5 us
  transfers between devices with their start and end apart: 18, of which 10 were waited for; matrix products, arithmetic and copies ran while one was open for 12% of the time, Pallas kernels for 0%

profile of v1, /device:TPU:0, one launch (start us, length us, event | category | flops | bytes accessed | tf_op | source)
XLA Modules:
  0.0 372.6 jit_solution(8088962765178282125)
XLA Ops:
  8.1 1.3 collective-permute-start.3
  9.4 5.5 %collective-permute-start.2 = (s32[128]{0:T(128)S(1)}, s32[128]{0:T(128)S(1)}, u32[]{:S(2)}, u32[]{:S(2)}) collective-permute-start(s32[128]{0:T(128)S(1)} %get-tuple-element.16), channel_id=1, source_target_pairs={{0,4},{4,8},{8,12},{12,16},{16,20},{20,24},{24,28},{1,5},{5,9},{9,... | collective-permute-start | bytes 1544 | tf_op jit(solution)/shard_map/ppermute | solution.py:17
  15.7 4.8 %collective-permute-start.4 = (bf16[128,128]{1,0:T(8,128)(2,1)S(1)}, bf16[128,128]{1,0:T(8,128)(2,1)S(1)}, u32[]{:S(2)}, u32[]{:S(2)}) collective-permute-start(bf16[128,128]{1,0:T(8,128)(2,1)S(1)} %get-tuple-element.11), channel_id=1, source_target_pairs={{0,4},{4,8},{8,12},{12,16},{16,20},{20,24},{24,28},{1,5},{5,9},{9,... | collective-permute-start | bytes 98312 | tf_op jit(solution)/shard_map/ppermute | solution.py:17
  20.5 1.3 collective-permute-start.5
  22.6 4.5 %collective-permute-start = (bf16[128,128]{1,0:T(8,128)(2,1)S(1)}, bf16[128,128]{1,0:T(8,128)(2,1)S(1)}, u32[]{:S(2)}, u32[]{:S(2)}) collective-permute-start(bf16[128,128]{1,0:T(8,128)(2,1)S(1)} %get-tuple-element.7), channel_id=1, source_target_pairs={{0,4},{4,8},{8,12},{12,16},{16,20},{20,24},{24,28},{1,5},{5,9},{9,... | collective-permute-start | bytes 98312 | tf_op jit(solution)/shard_map/ppermute | solution.py:17
  27.1 1.0 reshape.90
  28.2 1.0 reshape.87
  29.4 1.2 reshape.92
  31.6 1.3 collective-permute-start.1
  36.2 1.2 collective-permute-done.1
  40.6 8.7 %all_to_all.19 = bf16[4,128,256]{1,2,0:T(8,128)(2,1)S(1)} all-to-all(bf16[4,128,256]{1,2,0:T(8,128)(2,1)S(1)} %bitcast.41), channel_id=1, replica_groups=mesh['sp'=8,'tp'=4] {'tp'}, dimensions={0} | all-to-all | bytes 524288 | tf_op jit(solution)/shard_map/all_to_all | solution.py:76
  49.3 3.0 multiply_reduce_fusion
  54.7 2.5 collective-permute-start.6
  57.2 17.8 %collective-permute-done.6 = bf16[1408,256]{1,0:T(8,128)(2,1)S(1)} collective-permute-done((bf16[1408,256]{1,0:T(8,128)(2,1)S(1)}, bf16[1408,256]{1,0:T(8,128)(2,1)S(1)}, u32[]{:S(2)}, u32[]{:S(2)}) %collective-permute-start.6) | collective-permute-done | bytes 720928 | tf_op jit(solution)/shard_map/ppermute | solution.py:89
  75.0 23.3 %collective-permute-done.7 = bf16[1408,256]{1,0:T(8,128)(2,1)S(1)} collective-permute-done((bf16[1408,256]{1,0:T(8,128)(2,1)S(1)}, bf16[1408,256]{1,0:T(8,128)(2,1)S(1)}, u32[]{:S(2)}, u32[]{:S(2)}) %collective-permute-start.7) | collective-permute-done | bytes 720928 | tf_op jit(solution)/shard_map/ppermute | solution.py:89
  98.2 35.0 %collective-permute-done.8 = bf16[1408,256]{1,0:T(8,128)(2,1)S(1)} collective-permute-done((bf16[1408,256]{1,0:T(8,128)(2,1)S(1)}, bf16[1408,256]{1,0:T(8,128)(2,1)S(1)}, u32[]{:S(2)}, u32[]{:S(2)}) %collective-permute-start.8) | collective-permute-done | bytes 720928 | tf_op jit(solution)/shard_map/ppermute | solution.py:89
  134.1 32.2 %collective-permute-done.9 = bf16[1408,256]{1,0:T(8,128)(2,1)S(1)} collective-permute-done((bf16[1408,256]{1,0:T(8,128)(2,1)S(1)}, bf16[1408,256]{1,0:T(8,128)(2,1)S(1)}, u32[]{:S(2)}, u32[]{:S(2)}) %collective-permute-start.9) | collective-permute-done | bytes 720928 | tf_op jit(solution)/shard_map/ppermute | solution.py:89
  167.2 34.3 %collective-permute-done.10 = bf16[1408,256]{1,0:T(8,128)(2,1)S(1)} collective-permute-done((bf16[1408,256]{1,0:T(8,128)(2,1)S(1)}, bf16[1408,256]{1,0:T(8,128)(2,1)S(1)}, u32[]{:S(2)}, u32[]{:S(2)}) %collective-permute-start.10) | collective-permute-done | bytes 720928 | tf_op jit(solution)/shard_map/ppermute | solution.py:89
  202.3 23.5 %collective-permute-done.11 = bf16[1408,256]{1,0:T(8,128)(2,1)} collective-permute-done((bf16[1408,256]{1,0:T(8,128)(2,1)S(1)}, bf16[1408,256]{1,0:T(8,128)(2,1)}, u32[]{:S(2)}, u32[]{:S(2)}) %collective-permute-start.11) | collective-permute-done | bytes 720928 | tf_op jit(solution)/shard_map/ppermute | solution.py:89
  225.8 1.1 collective-permute-start.12
  226.9 25.5 %collective-permute-done.12 = bf16[1408,256]{1,0:T(8,128)(2,1)} collective-permute-done((bf16[1408,256]{1,0:T(8,128)(2,1)}, bf16[1408,256]{1,0:T(8,128)(2,1)}, u32[]{:S(2)}, u32[]{:S(2)}) %collective-permute-start.12) | collective-permute-done | bytes 720928 | tf_op jit(solution)/shard_map/ppermute | solution.py:89
  252.4 2.1 constant_dynamic-update-slice_fusion.15
  254.5 2.1 constant_dynamic-update-slice_fusion.14
  256.6 2.2 constant_dynamic-update-slice_fusion.13
  258.8 2.2 constant_dynamic-update-slice_fusion.12
  264.8 2.1 constant_dynamic-update-slice_fusion.7
  266.9 2.1 constant_dynamic-update-slice_fusion.6
  274.8 8.5 %fusion.34 = f32[512,1408]{1,0:T(8,128)} fusion(bf16[512,2048]{1,0:T(8,128)(2,1)} %all-gather.7.cloned.1.call-done, bf16[2048,1408]{1,0:T(8,128)(2,1)} %all-gather.9.cloned.1.call-done), kind=kOutput, calls=%fused_computation.71 | convolution fusion | flops 2952790016 | bytes 10747904 | tf_op jit(solution)/shard_map/dot_general | solution.py:82
  283.3 38.1 %all-gather.11.cloned.1.call-done = bf16[2048,1408]{1,0:T(8,128)(2,1)} async-done(((bf16[256,1408]{1,0:T(8,128)(2,1)}), bf16[2048,1408]{1,0:T(8,128)(2,1)}) %all-gather.11.cloned.1.call-update) | async-done | bytes 5767184 | tf_op jit(solution)/shard_map/all_gather | solution.py:85
  321.4 13.2 %fusion.3 = bf16[512,2048]{1,0:T(8,128)(2,1)} fusion(bf16[1408,4096]{1,0:T(8,128)(2,1)} %constant_dynamic-update-slice_fusion, s32[]{:T(128)S(6)} %select_n.27, bf16[512,2048]{1,0:T(8,128)(2,1)S(1)} %copy-done.10, bf16[2048,1408]{1,0:T(8,128)(2,1)} %all-gather.11.cloned.1.call-done, f32[512,1408]{1,0:T(8,128)} %fusion.34), kind=kOutput, calls=%fused_computation.7 | convolution fusion | flops 5910953984 | bytes 18612228 | tf_op jit(solution)/shard_map/dot_general | solution.py:94
  334.6 29.5 %reduce-scatter.2.cloned.1.call-done = bf16[128,2048]{1,0:T(8,128)(2,1)} async-done(((bf16[512,2048]{1,0:T(8,128)(2,1)}), bf16[128,2048]{1,0:T(8,128)(2,1)}) %reduce-scatter.2.cloned.1.call-update) | async-done | bytes 524304 | tf_op jit(solution)/shard_map/reduce_scatter | solution.py:93
  364.1 1.9 add_convert_fusion
  (84 shorter events, 25.1 us)
Async XLA Ops:
  6.5 30.9 %copy-start.7 = (bf16[512,128]{1,0:T(8,128)(2,1)S(1)}, bf16[512,128]{1,0:T(8,128)(2,1)}, u32[]{:S(2)}) copy-start(bf16[512,128]{1,0:T(8,128)(2,1)} %param.13) | copy-start | bytes 393220
  6.5 42.8 %all-gather.5.cloned.1.call-start = ((), (), s32[]{:S(2)}) async-start(), calls=%async_computation.2 | async-start | bytes 5242880 | tf_op jit(solution)/shard_map/all_gather | solution.py:41
  7.3 267.5 %all-gather.7.cloned.1.call-start = ((), (), s32[]{:S(2)}) async-start(), calls=%async_computation.3 | async-start | bytes 2621440 | tf_op jit(solution)/shard_map/all_gather | solution.py:79
  8.1 23.6 %collective-permute-start.3 = (s32[128]{0:T(128)S(1)}, s32[128]{0:T(128)S(1)}, u32[]{:S(2)}, u32[]{:S(2)}) collective-permute-start(s32[128]{0:T(128)S(1)} %get-tuple-element.17), channel_id=1, source_target_pairs={{4,0},{8,4},{12,8},{16,12},{20,16},{24,20},{28,24},{5,1},{9,5},{13... | collective-permute-start | bytes 1544 | tf_op jit(solution)/shard_map/ppermute | solution.py:20
  9.4 23.6 %collective-permute-start.2 = (s32[128]{0:T(128)S(1)}, s32[128]{0:T(128)S(1)}, u32[]{:S(2)}, u32[]{:S(2)}) collective-permute-start(s32[128]{0:T(128)S(1)} %get-tuple-element.16), channel_id=1, source_target_pairs={{0,4},{4,8},{8,12},{12,16},{16,20},{20,24},{24,28},{1,5},{5,9},{9,... | collective-permute-start | bytes 1544 | tf_op jit(solution)/shard_map/ppermute | solution.py:17
  15.7 18.9 %collective-permute-start.4 = (bf16[128,128]{1,0:T(8,128)(2,1)S(1)}, bf16[128,128]{1,0:T(8,128)(2,1)S(1)}, u32[]{:S(2)}, u32[]{:S(2)}) collective-permute-start(bf16[128,128]{1,0:T(8,128)(2,1)S(1)} %get-tuple-element.11), channel_id=1, source_target_pairs={{0,4},{4,8},{8,12},{12,16},{16,20},{20,24},{24,28},{1,5},{5,9},{9,... | collective-permute-start | bytes 98312 | tf_op jit(solution)/shard_map/ppermute | solution.py:17
  20.5 14.1 %collective-permute-start.5 = (bf16[128,128]{1,0:T(8,128)(2,1)S(1)}, bf16[128,128]{1,0:T(8,128)(2,1)S(1)}, u32[]{:S(2)}, u32[]{:S(2)}) collective-permute-start(bf16[128,128]{1,0:T(8,128)(2,1)S(1)} %get-tuple-element.12), channel_id=1, source_target_pairs={{4,0},{8,4},{12,8},{16,12},{20,16},{24,20},{28,24},{5,1},{9,5},{13... | collective-permute-start | bytes 98312 | tf_op jit(solution)/shard_map/ppermute | solution.py:20
  22.6 13.6 %collective-permute-start = (bf16[128,128]{1,0:T(8,128)(2,1)S(1)}, bf16[128,128]{1,0:T(8,128)(2,1)S(1)}, u32[]{:S(2)}, u32[]{:S(2)}) collective-permute-start(bf16[128,128]{1,0:T(8,128)(2,1)S(1)} %get-tuple-element.7), channel_id=1, source_target_pairs={{0,4},{4,8},{8,12},{12,16},{16,20},{20,24},{24,28},{1,5},{5,9},{9,... | collective-permute-start | bytes 98312 | tf_op jit(solution)/shard_map/ppermute | solution.py:17
  31.6 5.8 %collective-permute-start.1 = (bf16[128,128]{1,0:T(8,128)(2,1)S(1)}, bf16[128,128]{1,0:T(8,128)(2,1)S(1)}, u32[]{:S(2)}, u32[]{:S(2)}) collective-permute-start(bf16[128,128]{1,0:T(8,128)(2,1)S(1)} %get-tuple-element.8), channel_id=1, source_target_pairs={{4,0},{8,4},{12,8},{16,12},{20,16},{24,20},{28,24},{5,1},{9,5},{13... | collective-permute-start | bytes 98312 | tf_op jit(solution)/shard_map/ppermute | solution.py:20
  39.6 9.7 %copy-start.8 = (bf16[128,2048]{1,0:T(8,128)(2,1)S(1)}, bf16[128,2048]{1,0:T(8,128)(2,1)}, u32[]{:S(2)}) copy-start(bf16[128,2048]{1,0:T(8,128)(2,1)} %param.16) | copy-start | bytes 1572868
  40.6 11.8 %copy-start.9 = (f32[2048]{0:T(1024)S(1)}, f32[2048]{0:T(1024)}, u32[]{:S(2)}) copy-start(f32[2048]{0:T(1024)} %param.18) | copy-start | bytes 24580
  40.6 14.1 %copy-start = (bf16[1408,256]{1,0:T(8,128)(2,1)S(1)}, bf16[1408,256]{1,0:T(8,128)(2,1)}, u32[]{:S(2)}) copy-start(bf16[1408,256]{1,0:T(8,128)(2,1)} %param.21) | copy-start | bytes 2162692
  53.3 221.5 %all-gather.9.cloned.1.call-start = ((), (), s32[]{:S(2)}) async-start(), calls=%async_computation.4 | async-start | bytes 6488064 | tf_op jit(solution)/shard_map/all_gather | solution.py:84
  54.1 267.3 %all-gather.11.cloned.1.call-start = ((), (), s32[]{:S(2)}) async-start(), calls=%async_computation.5 | async-start | bytes 6488064 | tf_op jit(solution)/shard_map/all_gather | solution.py:85
  54.6 309.5 %reduce-scatter.2.cloned.1.call-start = ((), (), s32[]{:S(2)}) async-start(), calls=%async_computation.6 | async-start | bytes 2621440 | tf_op jit(solution)/shard_map/reduce_scatter | solution.py:93
  54.7 20.3 %collective-permute-start.6 = (bf16[1408,256]{1,0:T(8,128)(2,1)S(1)}, bf16[1408,256]{1,0:T(8,128)(2,1)S(1)}, u32[]{:S(2)}, u32[]{:S(2)}) collective-permute-start(bf16[1408,256]{1,0:T(8,128)(2,1)S(1)} %copy-done), channel_id=1, source_target_pairs={{0,4},{4,8},{8,12},{12,16},{16,20},{20,24},{24,28},{28,0},{1,5},{5... | collective-permute-start | bytes 2162696 | tf_op jit(solution)/shard_map/ppermute | solution.py:89
  75.0 23.3 %collective-permute-start.7 = (bf16[1408,256]{1,0:T(8,128)(2,1)S(1)}, bf16[1408,256]{1,0:T(8,128)(2,1)S(1)}, u32[]{:S(2)}, u32[]{:S(2)}) collective-permute-start(bf16[1408,256]{1,0:T(8,128)(2,1)S(1)} %collective-permute-done.6), channel_id=1, source_target_pairs={{0,4},{4,8},{8,12},{12,16},{16,20},{20,24},{24,28},{28,0},{1,5},{5... | collective-permute-start | bytes 2162696 | tf_op jit(solution)/shard_map/ppermute | solution.py:89
  98.2 35.0 %collective-permute-start.8 = (bf16[1408,256]{1,0:T(8,128)(2,1)S(1)}, bf16[1408,256]{1,0:T(8,128)(2,1)S(1)}, u32[]{:S(2)}, u32[]{:S(2)}) collective-permute-start(bf16[1408,256]{1,0:T(8,128)(2,1)S(1)} %collective-permute-done.7), channel_id=1, source_target_pairs={{0,4},{4,8},{8,12},{12,16},{16,20},{20,24},{24,28},{28,0},{1,5},{5... | collective-permute-start | bytes 2162696 | tf_op jit(solution)/shard_map/ppermute | solution.py:89
  133.2 0.9 copy-start.1
  134.1 32.3 %collective-permute-start.9 = (bf16[1408,256]{1,0:T(8,128)(2,1)S(1)}, bf16[1408,256]{1,0:T(8,128)(2,1)S(1)}, u32[]{:S(2)}, u32[]{:S(2)}) collective-permute-start(bf16[1408,256]{1,0:T(8,128)(2,1)S(1)} %collective-permute-done.8), channel_id=1, source_target_pairs={{0,4},{4,8},{8,12},{12,16},{16,20},{20,24},{24,28},{28,0},{1,5},{5... | collective-permute-start | bytes 2162696 | tf_op jit(solution)/shard_map/ppermute | solution.py:89
  166.3 0.9 copy-start.3
  167.2 34.3 %collective-permute-start.10 = (bf16[1408,256]{1,0:T(8,128)(2,1)S(1)}, bf16[1408,256]{1,0:T(8,128)(2,1)S(1)}, u32[]{:S(2)}, u32[]{:S(2)}) collective-permute-start(bf16[1408,256]{1,0:T(8,128)(2,1)S(1)} %collective-permute-done.9), channel_id=1, source_target_pairs={{0,4},{4,8},{8,12},{12,16},{16,20},{20,24},{24,28},{28,0},{1,5},{5... | collective-permute-start | bytes 2162696 | tf_op jit(solution)/shard_map/ppermute | solution.py:89
  201.5 0.9 copy-start.5
  202.3 23.5 %collective-permute-start.11 = (bf16[1408,256]{1,0:T(8,128)(2,1)S(1)}, bf16[1408,256]{1,0:T(8,128)(2,1)}, u32[]{:S(2)}, u32[]{:S(2)}) collective-permute-start(bf16[1408,256]{1,0:T(8,128)(2,1)S(1)} %collective-permute-done.10), channel_id=1, source_target_pairs={{0,4},{4,8},{8,12},{12,16},{16,20},{20,24},{24,28},{28,0},{1,5},{5... | collective-permute-start | bytes 2162696 | tf_op jit(solution)/shard_map/ppermute | solution.py:89
  225.8 26.6 %collective-permute-start.12 = (bf16[1408,256]{1,0:T(8,128)(2,1)}, bf16[1408,256]{1,0:T(8,128)(2,1)}, u32[]{:S(2)}, u32[]{:S(2)}) collective-permute-start(bf16[1408,256]{1,0:T(8,128)(2,1)} %collective-permute-done.11), channel_id=1, source_target_pairs={{0,4},{4,8},{8,12},{12,16},{16,20},{20,24},{24,28},{28,0},{1,5},{5... | collective-permute-start | bytes 2162696 | tf_op jit(solution)/shard_map/ppermute | solution.py:89
  226.9 34.0 %copy-start.2 = (bf16[1408,256]{1,0:T(8,128)(2,1)S(1)}, bf16[1408,256]{1,0:T(8,128)(2,1)}, u32[]{:S(2)}) copy-start(bf16[1408,256]{1,0:T(8,128)(2,1)} %copy-done.1) | copy-start | bytes 2162692
  256.6 12.4 %copy-start.6 = (bf16[1408,256]{1,0:T(8,128)(2,1)S(1)}, bf16[1408,256]{1,0:T(8,128)(2,1)}, u32[]{:S(2)}) copy-start(bf16[1408,256]{1,0:T(8,128)(2,1)} %copy-done.5) | copy-start | bytes 2162692
  258.8 11.2 %copy-start.4 = (bf16[1408,256]{1,0:T(8,128)(2,1)S(1)}, bf16[1408,256]{1,0:T(8,128)(2,1)}, u32[]{:S(2)}) copy-start(bf16[1408,256]{1,0:T(8,128)(2,1)} %copy-done.3) | copy-start | bytes 2162692
  274.8 46.6 %copy-start.10 = (bf16[512,2048]{1,0:T(8,128)(2,1)S(1)}, bf16[512,2048]{1,0:T(8,128)(2,1)}, u32[]{:S(2)}) copy-start(bf16[512,2048]{1,0:T(8,128)(2,1)} %all-gather.7.cloned.1.call-done) | copy-start | bytes 6291460
Sparse Core Ops, SparseCore 0:
  8.9 37.1 all-gather.4
  53.4 22.7 all-gather.6
  78.4 132.7 all-gather.8
  213.2 108.1 all-gather.10
  334.8 29.3 reduce-scatter.1
